TPU v7x, 32 devices: a whole 2x2x4 slice. The times are simulated.
32 devices in a mesh: ep: 8 (over z, x), tp: 4 (over y, core).
Axes of the slice: x: 2, y: 2, z: 4, core: 2. Of those that a mesh axis runs over, the one named last changes fastest.
Arguments:
- gate_branch: bfloat16 [4096, 2048], P(('ep', 'tp')), may hold values from -8 to 8
- rec_branch: bfloat16 [4096, 2048], P(('ep', 'tp')), may hold values from -6 to 6
- conv_weight: float32 [4, 2048], replicated, may hold values from -3 to 3
- gate_a: bfloat16 [8, 256, 256], replicated, may hold values from -0.375 to 0.375
- gate_x: bfloat16 [8, 256, 256], replicated, may hold values from -0.375 to 0.375
- decay_param: float32 [2048], replicated, as said below
- decay_shift: float32 [4096], P(('ep', 'tp')), may hold values from -0.6 to 0
- tokens: bfloat16 [4096, 2048], P(('ep', 'tp')), may hold values from -6 to 6
- routes: int32 [4096, 2], P(('ep', 'tp')), may hold values from 0 to 7, all different within a row; in each aligned block of 128 rows (0 to 127, 128 to 255, ...) at most 40 rows name the same one
- route_weight: float32 [4096, 2], P(('ep', 'tp')), may hold values from 0.1 to 0.9
- norm_gain: float32 [2048], replicated, may hold values from 0.1 to 1.9
- w_gate: bfloat16 [8, 2048, 3584], P('ep', None, 'tp'), may hold values from -0.125 to 0.125
- w_up: bfloat16 [8, 2048, 3584], P('ep', None, 'tp'), may hold values from -0.125 to 0.125
- w_down: bfloat16 [8, 3584, 2048], P('ep', 'tp'), may hold values from -0.09375 to 0.09375
Outputs:
- mixed_out: bfloat16 [4096, 2048], P(('ep', 'tp'))
- expert_out: bfloat16 [4096, 2048], P(('ep', 'tp'))
Inputs may be any that keep to these rules, and one draw needn't show every extreme that they name: `routes`: in each aligned block of 128 rows (the rows of one device) no expert is named more than 40 times, and some block names some expert exactly 40 times; the experts of one row differ. 8 softplus(-decay_param) lies between 0.2 / 4096 and 0.07.
All inputs are finite; a program needn't handle non-finite values.
Results may differ from a plain program's by a relative error of at most 0.012.
Values may be sent and summed in bfloat16 or wider, within the bound.
A program may use at most 128 MiB of HBM per device.

v0:
```python
import math

import jax
import jax.numpy as jnp
from jax import lax
from jax.sharding import PartitionSpec as P

EPSILON = 1e-05


def passed_along(block, axis, distance):
    devices = range(lax.axis_size(axis))
    route = [(i - distance, i) for i in devices if i - distance in devices]
    return lax.ppermute(block, axis, route)


def prefix(part, axis, combine, identity):
    place = lax.axis_index(axis)
    gathered = jax.tree.map(lambda a: lax.all_gather(a, axis), part)
    state = jax.tree.map(lambda a, e: jnp.zeros_like(a) + jnp.asarray(e, a.dtype), part, identity)

    def one(lap, state):
        return combine(
            state, jax.tree.map(lambda a: lax.dynamic_index_in_dim(a, lap, 0, False), gathered)
        )

    return lax.fori_loop(0, place, one, state)


def pair_combine(earlier, later):
    return (earlier[0] * later[0], later[0] * earlier[1] + later[1])


def short_conv(previous, current, conv_weight):
    tap_count = conv_weight.shape[0]
    row_count = current.shape[0]
    padded = jnp.concatenate([previous, current], 0)
    summed = jnp.zeros(current.shape, jnp.float32)
    for tap_index in range(tap_count):
        summed = summed + conv_weight[tap_index] * padded[tap_index : tap_index + row_count].astype(
            jnp.float32
        )
    return summed.astype(jnp.bfloat16)


def mixer_gates(conv_rows, gate_a, gate_x, decay_rate, shift_rows):
    row_count, width_all = conv_rows.shape
    block_count, block_width = (gate_a.shape[0], gate_a.shape[1])
    split_rows = conv_rows.reshape(row_count, block_count, block_width)
    pre_a = jnp.einsum("rnc,ncd->rnd", split_rows, gate_a, preferred_element_type=jnp.float32)
    pre_x = jnp.einsum("rnc,ncd->rnd", split_rows, gate_x, preferred_element_type=jnp.float32)
    recur_gate = jax.nn.sigmoid(pre_a.reshape(row_count, width_all))
    input_gate = jax.nn.sigmoid(pre_x.reshape(row_count, width_all))
    log_a = -decay_rate[None, :] * recur_gate + shift_rows[:, None]
    drive = jnp.sqrt(-jnp.expm1(2.0 * log_a)) * input_gate * conv_rows.astype(jnp.float32)
    return (log_a, drive)


def blocked_recurrence(decay, drive):
    row_count, width_all = decay.shape
    group = math.gcd(row_count, 8)
    block_count = row_count // group
    decay_blocks = decay.reshape(block_count, group, width_all)
    drive_blocks = drive.reshape(block_count, group, width_all)
    factors = [decay_blocks[:, 0]]
    states = [drive_blocks[:, 0]]
    for inner in range(1, group):
        factors.append(factors[-1] * decay_blocks[:, inner])
        states.append(decay_blocks[:, inner] * states[-1] + drive_blocks[:, inner])
    factor_inner = jnp.stack(factors, 1)
    state_inner = jnp.stack(states, 1)

    def carry_step(carried, totals):
        return (pair_combine(carried, totals), carried)

    start = (jnp.ones((width_all,), jnp.float32), jnp.zeros((width_all,), jnp.float32))
    _, before = lax.scan(carry_step, start, (factors[-1], states[-1]))
    factor_all = factor_inner * before[0][:, None, :]
    state_all = state_inner + factor_inner * before[1][:, None, :]
    return (factor_all.reshape(row_count, width_all), state_all.reshape(row_count, width_all))


def layer_scale(rows_in, norm_gain):
    values = rows_in.astype(jnp.float32)
    center = jnp.mean(values, -1, keepdims=True)
    spread = jnp.mean(jnp.square(values - center), -1, keepdims=True)
    return ((values - center) * lax.rsqrt(spread + EPSILON) * norm_gain).astype(jnp.bfloat16)


def slot_numbers(routes, block_rows, expert_count):
    row_count, top_count = routes.shape
    onehot = (routes[:, :, None] == jnp.arange(expert_count, dtype=jnp.int32)).astype(jnp.int32)
    ranked = (
        jnp.cumsum(
            onehot.reshape(row_count // block_rows, block_rows * top_count, expert_count), axis=1
        )
        - 1
    )
    return jnp.sum(ranked.reshape(row_count, top_count, expert_count) * onehot, -1)


def expert_hidden(rows_in, gate_part, up_part):
    return (
        jax.nn.silu(jnp.dot(rows_in, gate_part, preferred_element_type=jnp.float32))
        * jnp.dot(rows_in, up_part, preferred_element_type=jnp.float32)
    ).astype(jnp.bfloat16)


def shards(
    gate_branch,
    rec_branch,
    conv_weight,
    gate_a,
    gate_x,
    decay_param,
    decay_shift,
    tokens,
    routes,
    route_weight,
    norm_gain,
    w_gate,
    w_up,
    w_down,
):
    tap_count = conv_weight.shape[0]
    row_count, width_all = rec_branch.shape
    previous = passed_along(rec_branch[row_count - (tap_count - 1) :], ("ep", "tp"), 1)
    conv_rows = short_conv(previous, rec_branch, conv_weight)
    decay_rate = 8.0 * jax.nn.softplus(-decay_param)
    log_a, drive = mixer_gates(conv_rows, gate_a, gate_x, decay_rate, decay_shift)
    factor, local_state = blocked_recurrence(jnp.exp(log_a), drive)
    identity = (jnp.ones((width_all,), jnp.float32), jnp.zeros((width_all,), jnp.float32))
    carried = prefix((factor[-1], local_state[-1]), ("ep", "tp"), pair_combine, identity)
    states = local_state + factor * carried[1][None, :]
    mixed_out = (states * jax.nn.gelu(gate_branch.astype(jnp.float32), approximate=True)).astype(
        jnp.bfloat16
    )
    ep_count = lax.axis_size("ep")
    block_rows, top_count = routes.shape
    capacity = max(2, block_rows * top_count * 5 // (4 * ep_count))
    normed = layer_scale(tokens, norm_gain)
    slots = slot_numbers(routes, block_rows, ep_count)
    row_ids = jnp.broadcast_to(jnp.arange(block_rows, dtype=jnp.int32)[:, None], routes.shape)
    flat = routes * capacity + slots
    table = jnp.full((ep_count * capacity,), block_rows, jnp.int32)
    table = table.at[flat.reshape(-1)].set(row_ids.reshape(-1))
    outgoing = jnp.take(normed, table, axis=0, mode="fill", fill_value=0)
    outgoing = outgoing.reshape(ep_count, capacity, width_all)
    arrived = lax.all_to_all(outgoing, "ep", split_axis=0, concat_axis=0, tiled=True)
    hidden = expert_hidden(
        lax.all_gather(arrived.reshape(-1, width_all), "tp", axis=0, tiled=True), w_gate[0], w_up[0]
    )
    route_out = lax.psum_scatter(
        jnp.dot(hidden, w_down[0], preferred_element_type=jnp.float32).astype(jnp.bfloat16),
        "tp",
        scatter_dimension=0,
        tiled=True,
    )
    returned = lax.all_to_all(
        route_out.reshape(ep_count, capacity, width_all),
        "ep",
        split_axis=0,
        concat_axis=0,
        tiled=True,
    )
    returned = returned.reshape(ep_count * capacity, width_all)
    picked = jnp.take(returned, flat.reshape(-1), axis=0).astype(jnp.float32)
    picked = picked.reshape(block_rows, top_count, width_all)
    expert_out = jnp.sum(picked * route_weight[:, :, None], axis=1).astype(jnp.bfloat16)
    return (mixed_out, expert_out)


def solution(mesh):
    in_specs = (
        P(("ep", "tp"), None),
        P(("ep", "tp"), None),
        P(),
        P(),
        P(),
        P(),
        P(("ep", "tp")),
        P(("ep", "tp"), None),
        P(("ep", "tp"), None),
        P(("ep", "tp"), None),
        P(),
        P("ep", None, "tp"),
        P("ep", None, "tp"),
        P("ep", "tp", None),
    )
    out_specs = (P(("ep", "tp"), None), P(("ep", "tp"), None))
    return jax.shard_map(shards, mesh=mesh, in_specs=in_specs, out_specs=out_specs, check_vma=False)
```

profile of v0, /device:TPU:0, one launch (start us, length us, event | category | flops | bytes accessed | tf_op | source)
XLA Modules:
  0.0 316.3 jit_solution(2899223735490568376)
XLA Ops:
  10.5 1.4 scatter_custom_fusion
  12.0 1.2 convert_reduce_fusion
  13.2 1.3 fusion.14
  14.6 1.4 fusion.16
  16.0 2.4 gather_fusion
  18.7 38.6 %all_to_all.10 = bf16[8,40,2048]{2,1,0:T(8,128)(2,1)} all-to-all(bf16[8,40,2048]{2,1,0:T(8,128)(2,1)S(1)} %broadcast_select_fusion.3), channel_id=1, replica_groups=mesh['ep'=8,'tp'=4] {'ep'}, dimensions={0} | all-to-all | bytes 2621440 | tf_op jit(solution)/shard_map/all_to_all | solution.py:149
  57.7 1.5 collective-permute-start
  61.7 2.1 add_convert_fusion
  64.6 1.3 copy.53
  66.6 3.0 fusion.7
  69.6 2.5 copy.55
  72.1 3.2 %fusion.24 = f32[128,2048]{0,1:T(8,128)} fusion(f32[128,8,256]{0,2,1:T(8,128)} %copy.55, f32[128,8,256]{0,2,1:T(8,128)S(1)} %copy-done.2, bf16[128,2048]{0,1:T(8,128)(2,1)} %copy-done.3, f32[128]{0:T(128)S(1)} %copy-done.9, f32[2048]{0:T(1024)S(1)} %fusion.33), kind=kLoop, calls=%fused_computation.53 | loop fusion | flops 1835008 | bytes 3678720 | tf_op jit(solution)/shard_map/mul | solution.py:55
  75.3 1.6 copy.56
  76.8 1.1 div.30
  78.0 1.4 add_exponential_fusion
  79.4 17.5 %all-gather.4.cloned.1.call-done = bf16[1280,2048]{1,0:T(8,128)(2,1)} async-done(((bf16[320,2048]{1,0:T(8,128)(2,1)}), bf16[1280,2048]{1,0:T(8,128)(2,1)}) %all-gather.4.cloned.1.call-update) | async-done | bytes 5242896 | tf_op jit(solution)/shard_map/all_gather | solution.py:151
  96.9 9.9 %fusion.2 = f32[1280,896]{1,0:T(8,128)} fusion(bf16[1280,2048]{1,0:T(8,128)(2,1)} %all-gather.4.cloned.1.call-done, bf16[1,2048,896]{2,1,0:T(8,128)(2,1)} %param.29), kind=kOutput, calls=%fused_computation.15 | convolution fusion | flops 4697620480 | bytes 13500416 | tf_op jit(solution)/shard_map/dot_general | solution.py:104
  106.8 17.5 %convolution_convert_fusion = bf16[1280,2048]{1,0:T(8,128)(2,1)} fusion(bf16[1,896,2048]{2,1,0:T(8,128)(2,1)} %param.31, f32[1280,896]{1,0:T(8,128)} %fusion.2, bf16[1280,2048]{1,0:T(8,128)(2,1)} %all-gather.4.cloned.1.call-done, bf16[1,2048,896]{2,1,0:T(8,128)(2,1)} %param.30), kind=kOutput, calls=%fused_computation.11 | convolution fusion | flops 9404743680 | bytes 22413312 | tf_op jit(solution)/shard_map/dot_general | solution.py:154
  124.3 2.2 slice_add_fusion
  126.6 3.0 stack.4
  129.6 1.6 slice_multiply_fusion
  131.2 3.9 %stack.5 = f32[16,8,2048]{2,1,0:T(8,128)} concatenate(f32[16,1,2048]{2,1,0:T(1,128)} %get-tuple-element.163, f32[16,1,2048]{2,1,0:T(1,128)} %get-tuple-element.147, f32[16,1,2048]{2,1,0:T(1,128)} %get-tuple-element.146, f32[16,1,2048]{2,1,0:T(1,128)} %get-tuple-element.145, f32[16,1,2048]{2,1,0:T(1,128)} %get-tuple-element.144, f32[16,1,2048]{2,1,0:T(1,128)} %get-tuple-element.143, ...), dimensions={1} | concatenate | bytes 2097152 | tf_op jit(solution)/shard_map/stack | solution.py:70
  135.2 48.4 %while.30 = (s32[]{:T(128)}, f32[2048]{0:T(1024)S(1)}, f32[2048]{0:T(1024)S(1)}, f32[16,2048]{1,0:T(8,128)}, f32[16,2048]{1,0:T(8,128)}, /*index=5*/f32[16,2048]...) while((s32[]{:T(128)}, f32[2048]{0:T(1024)S(1)}, f32[2048]{0:T(1024)S(1)}, ...), condition=%wide.region_1.2_spmd.clone, body=%wide.region_0.1_spmd.clone.sunk | while | flops 10243 | bytes 131187 | solution.py:77
  135.3 1.5 dynamic_update_slice.12
  136.8 1.5 dynamic_update_slice.11
  138.3 1.5 dynamic_update_slice.12
  139.8 1.5 dynamic_update_slice.11
  141.3 1.5 dynamic_update_slice.12
  142.8 1.5 dynamic_update_slice.11
  144.3 1.5 dynamic_update_slice.12
  145.9 1.5 dynamic_update_slice.11
  147.4 1.5 dynamic_update_slice.12
  148.9 1.5 dynamic_update_slice.11
  150.4 1.5 dynamic_update_slice.12
  151.9 1.5 dynamic_update_slice.11
  153.4 1.5 dynamic_update_slice.12
  154.9 1.5 dynamic_update_slice.11
  156.5 1.5 dynamic_update_slice.12
  157.9 1.5 dynamic_update_slice.11
  159.5 1.5 dynamic_update_slice.12
  161.0 1.5 dynamic_update_slice.11
  162.5 1.5 dynamic_update_slice.12
  164.0 1.5 dynamic_update_slice.11
  165.5 1.5 dynamic_update_slice.12
  167.0 1.5 dynamic_update_slice.11
  168.5 1.5 dynamic_update_slice.12
  170.0 1.5 dynamic_update_slice.11
  171.5 1.5 dynamic_update_slice.12
  173.0 1.5 dynamic_update_slice.11
  174.6 1.5 dynamic_update_slice.12
  176.1 1.5 dynamic_update_slice.11
  177.6 1.5 dynamic_update_slice.12
  179.1 1.5 dynamic_update_slice.11
  180.6 1.5 dynamic_update_slice.12
  182.1 1.5 dynamic_update_slice.11
  183.6 1.6 multiply_bitcast_fusion
  185.2 1.0 copy-done.1
  186.1 41.4 %all-gather.1 = f32[32,1,2048]{2,1,0:T(1,128)S(1)} all-gather(f32[1,1,2048]{2,1,0:T(1,128)S(1)} %slice_bitcast_fusion), channel_id=1, replica_groups=mesh['ep'=8,'tp'=4] {'ep','tp'}, dimensions={0}, use_global_device_ids=true | all-gather | bytes 270336 | tf_op jit(solution)/shard_map/all_gather | solution.py:19
  228.3 37.4 %all-gather = f32[32,1,2048]{2,1,0:T(1,128)S(1)} all-gather(f32[1,1,2048]{2,1,0:T(1,128)S(1)} %slice_bitcast_fusion.1), channel_id=1, replica_groups=mesh['ep'=8,'tp'=4] {'ep','tp'}, dimensions={0}, use_global_device_ids=true | all-gather | bytes 270336 | tf_op jit(solution)/shard_map/all_gather | solution.py:19
  266.5 3.6 %all-to-all-start.1 = ((bf16[8,40,2048]{2,1,0:T(8,128)(2,1)}), bf16[8,40,2048]{2,1,0:T(8,128)(2,1)S(1)}, u32[]{:S(2)}, u32[]{:S(2)}) async-start(bf16[8,40,2048]{2,1,0:T(8,128)(2,1)} %bitcast.118), calls=%async_computation.2 | async-start | bytes 2621440 | tf_op jit(solution)/shard_map/all_to_all | solution.py:159
  270.1 2.6 fusion.23
  272.7 29.4 %all-to-all-done.1 = bf16[8,40,2048]{2,1,0:T(8,128)(2,1)S(1)} async-done(((bf16[8,40,2048]{2,1,0:T(8,128)(2,1)}), bf16[8,40,2048]{2,1,0:T(8,128)(2,1)S(1)}, u32[]{:S(2)}, u32[]{:S(2)}) %all-to-all-start.1) | async-done | bytes 1310752 | tf_op jit(solution)/shard_map/all_to_all | solution.py:159
  302.1 1.6 gather_fusion.1
  304.5 4.9 %multiply_reduce_fusion = bf16[128,2048]{1,0:T(8,128)(2,1)} fusion(bf16[128,2,2048]{2,1,0:T(2,128)(2,1)S(1)} %gather.15, pred[128,2]{1,0:T(8,128)(4,1)S(1)} %copy-done.6, f32[128,2]{1,0:T(8,128)S(1)} %copy-done.5), kind=kLoop, calls=%fused_computation.17 | loop fusion | flops 1835008 | bytes 1574144 | tf_op jit(solution)/shard_map/reduce_sum | solution.py:169
  (105 shorter events, 10.6 us)
Async XLA Ops:
  7.2 56.7 %copy-start = (bf16[8,256,256]{2,1,0:T(8,128)(2,1)S(1)}, bf16[8,256,256]{2,1,0:T(8,128)(2,1)}, u32[]{:S(2)}) copy-start(bf16[8,256,256]{2,1,0:T(8,128)(2,1)} %param.21) | copy-start | bytes 3145732
  7.2 89.7 %all-gather.4.cloned.1.call-start = ((), (), s32[]{:S(2)}) async-start(), calls=%async_computation.3 | async-start | bytes 6553600 | tf_op jit(solution)/shard_map/all_gather | solution.py:151
  18.5 38.9 %copy-start.4 = (bf16[128,2048]{1,0:T(8,128)(2,1)S(1)}, bf16[128,2048]{1,0:T(8,128)(2,1)}, u32[]{:S(2)}) copy-start(bf16[128,2048]{1,0:T(8,128)(2,1)} %param.19) | copy-start | bytes 1572868
  18.5 40.7 %copy-start.8 = (f32[2048]{0:T(1024)S(1)}, f32[2048]{0:T(1024)}, u32[]{:S(2)}) copy-start(f32[2048]{0:T(1024)} %param.23) | copy-start | bytes 24580
  18.5 40.7 %copy-start.7 = (f32[4,2048]{1,0:T(4,128)S(1)}, f32[4,2048]{1,0:T(4,128)}, u32[]{:S(2)}) copy-start(f32[4,2048]{1,0:T(4,128)} %param.20) | copy-start | bytes 98308
  18.5 41.7 %copy-start.9 = (f32[128]{0:T(128)S(1)}, f32[128]{0:T(128)}, u32[]{:S(2)}) copy-start(f32[128]{0:T(128)} %param.24) | copy-start | bytes 1540
  18.5 42.5 %copy-start.10 = (f32[128,2]{0,1:T(2,128)S(1)}, f32[128,2]{0,1:T(2,128)}, u32[]{:S(2)}) copy-start(f32[128,2]{0,1:T(2,128)} %param.27) | copy-start | bytes 3076
  57.3 209.2 %reduce-scatter.2.cloned.1.call-start = ((), (), s32[]{:S(2)}) async-start(), calls=%async_computation.4 | async-start | bytes 6553600 | tf_op jit(solution)/shard_map/reduce_scatter | solution.py:153
  57.7 4.1 %collective-permute-start = (bf16[3,2048]{0,1:T(8,128)(2,1)S(1)}, bf16[3,2048]{0,1:T(8,128)(2,1)S(1)}, u32[]{:S(2)}, u32[]{:S(2)}) collective-permute-start(bf16[3,2048]{0,1:T(8,128)(2,1)S(1)} %copy.49), channel_id=1, source_target_pairs={{0,1},{1,2},{2,3},{3,4},{4,5},{5,6},{6,7},{7,8},{8,9},{9,10},{10,1... | collective-permute-start | bytes 36872 | tf_op jit(solution)/shard_map/ppermute | solution.py:14
  63.8 0.8 copy-start.3
  66.6 5.5 %copy-start.2 = (f32[128,8,256]{0,2,1:T(8,128)S(1)}, f32[128,8,256]{0,2,1:T(8,128)}, u32[]{:S(2)}) copy-start(f32[128,8,256]{0,2,1:T(8,128)} %copy.53) | copy-start | bytes 3145732
  185.1 1.0 copy-start.1
  266.5 35.7 %all-to-all-start.1 = ((bf16[8,40,2048]{2,1,0:T(8,128)(2,1)}), bf16[8,40,2048]{2,1,0:T(8,128)(2,1)S(1)}, u32[]{:S(2)}, u32[]{:S(2)}) async-start(bf16[8,40,2048]{2,1,0:T(8,128)(2,1)} %bitcast.118), calls=%async_computation.2 | async-start | bytes 2621440 | tf_op jit(solution)/shard_map/all_to_all | solution.py:159
  302.1 2.4 copy-start.5
  302.1 2.4 copy-start.6
Sparse Core Ops, SparseCore 0:
  57.4 39.4 all-gather.3
  124.5 51.4 reduce-scatter.1
where the time goes:
time: 320 us; the launch traced here: 316 us
  blocking collectives  117 us (37%)
  local copies, waits for them, and re-layouts  75.2 us (24%)
  waiting for transfers between devices  46.9 us (15%)
  matrix products  30.9 us (10%)
  other arithmetic  26 us (8%)
  between operations  14.4 us (4%)
  starting transfers between devices  5.15 us (2%)
    all_gather x2, blocking collectives, prefix(): gathered = jax.tree.map(lambda a: lax.all_gather(a, axis), part)  78.7 us
    dynamic_update_slice x32, local copies, waits for them, and re-layouts, blocked_recurrence(): _, before = lax.scan(carry_step, start, (factors[-1], states[-1]))  47.7 us
    all_to_all x1, blocking collectives, shards(): lax.all_to_all(outgoing, 'ep', split_axis=0, concat_axis=0, tiled=True)  38.6 us
    all_to_all x1, waiting for transfers between devices, shards(): lax.all_to_all(route_out.reshape(ep_count, capacity, width_all), 'ep', sp...  29.4 us
    dot_general x1, matrix products, shards(): jnp.dot(hidden, w_down[0], preferred_element_type=jnp.float32)  17.5 us
    all_gather x1, waiting for transfers between devices, shards(): lax.all_gather(arrived.reshape(-1, width_all), 'tp', axis=0, tiled=True)  17.5 us
    dot_general x1, matrix products, expert_hidden(): jnp.dot(rows_in, gate_part, preferred_element_type=jnp.float32)  9.94 us
  transfers between devices with their start and end apart: 4, of which 2 were waited for; matrix products, arithmetic and copies ran while one was open for 27% of the time, Pallas kernels for 0%

commit v1 on v0

v1 whole, which is shorter than its diff:
```python
import functools

import jax
import jax.numpy as jnp
from jax import lax
from jax.experimental import pallas as pl
from jax.experimental.pallas import tpu as pltpu
from jax.sharding import PartitionSpec as P

EPSILON = 1e-05
MESH = pl.DeviceIdType.MESH


def passed_along(block, axis, distance):
    devices = range(lax.axis_size(axis))
    route = [(i - distance, i) for i in devices if i - distance in devices]
    return lax.ppermute(block, axis, route)


def slot_numbers(routes, block_rows, expert_count):
    row_count, top_count = routes.shape
    onehot = (routes[:, :, None] == jnp.arange(expert_count, dtype=jnp.int32)).astype(jnp.int32)
    ranked = (
        jnp.cumsum(
            onehot.reshape(row_count // block_rows, block_rows * top_count, expert_count), axis=1
        )
        - 1
    )
    return jnp.sum(ranked.reshape(row_count, top_count, expert_count) * onehot, -1)


def shifted(values, distance, fill):
    lead = jnp.full((distance, values.shape[1]), fill, values.dtype)
    return jnp.concatenate([lead, values[: values.shape[0] - distance]], 0)


def mixer_kernel(prev_ref, rec_ref, conv_ref, ga_ref, gx_ref, rate_ref, shift_ref, f_ref, s_ref):
    rows = rec_ref.shape[0]
    taps = conv_ref.shape[0]
    lead = prev_ref.shape[0]
    padded = jnp.concatenate([prev_ref[...], rec_ref[...].astype(jnp.float32)], 0)
    first = lead - (taps - 1)
    summed = jnp.zeros(rec_ref.shape, jnp.float32)
    for tap in range(taps):
        summed = summed + conv_ref[tap : tap + 1, :] * padded[first + tap : first + tap + rows]
    conv_rows = summed.astype(jnp.bfloat16)
    recur = jax.nn.sigmoid(jnp.dot(conv_rows, ga_ref[0], preferred_element_type=jnp.float32))
    gate = jax.nn.sigmoid(jnp.dot(conv_rows, gx_ref[0], preferred_element_type=jnp.float32))
    log_a = -rate_ref[...] * recur + shift_ref[...]
    twice = 2.0 * log_a
    series = twice * (1.0 + twice * (0.5 + twice * (1.0 / 6.0 + twice * (1.0 / 24.0))))
    lost = jnp.where(twice > -0.03, -series, 1.0 - jnp.exp(twice))
    state = jnp.sqrt(lost) * gate * conv_rows.astype(jnp.float32)
    factor = jnp.exp(log_a)
    distance = 1
    while distance < rows:
        state = factor * shifted(state, distance, 0.0) + state
        factor = factor * shifted(factor, distance, 1.0)
        distance *= 2
    f_ref[...] = factor
    s_ref[...] = state


def local_mixer(prev, rec, conv_weight, gate_a, gate_x, rate, shift):
    rows, width = rec.shape
    blocks, wide = gate_a.shape[:2]
    col = lambda r: pl.BlockSpec((r, wide), lambda i: (0, i))
    mat = pl.BlockSpec((1, wide, wide), lambda i: (i, 0, 0))
    return pl.pallas_call(
        mixer_kernel,
        grid=(blocks,),
        in_specs=[col(prev.shape[0]), col(rows), col(conv_weight.shape[0]), mat, mat, col(1),
                  pl.BlockSpec((rows, 1), lambda i: (0, 0))],
        out_specs=[col(rows), col(rows)],
        out_shape=[jax.ShapeDtypeStruct((rows, width), jnp.float32)] * 2,
    )(prev, rec, conv_weight, gate_a, gate_x, rate, shift)


def expert_kernel(n, m, slot, tok_ref, gain_ref, flat_ref, flat_t_ref, weight_ref, tot_ref,
                  wg_hbm, wu_hbm, wd_hbm, out_ref, carry_ref,
                  wg, wu, wd, going, rows, half, back, tp_tot, grp, ep_tot,
                  w_sem, d_s, d_r, a_s, a_r, b_s, b_r, c_s, c_r, ra_s, ra_r, rb_s, rb_r,
                  q_s, q_r, t_s, t_r, e_s, e_r):
    e = lax.axis_index("ep")
    t = lax.axis_index("tp")
    pa = t + 1 - 2 * (t % 2)
    pb = (t + m // 2) % m
    pd = (pa + m // 2) % m
    loads = [pltpu.make_async_copy(h, v, w_sem.at[i])
             for i, (h, v) in enumerate(((wg_hbm, wg), (wu_hbm, wu), (wd_hbm, wd)))]
    for load in loads:
        load.start()

    barrier = pltpu.get_barrier_semaphore()

    def greet(k, _):
        pl.semaphore_signal(barrier, inc=1, device_id=((e + k) % n, t), device_id_type=MESH)
        return 0

    lax.fori_loop(1, n, greet, 0)
    for d in range(1, m):
        pl.semaphore_signal(barrier, inc=1, device_id=(e, (t + d) % m), device_id_type=MESH)

    def at(r, s, q):
        return r.at[s, pl.ds(pl.multiple_of(q * slot, slot), slot), :]

    def part(s, q):
        return rows[s, pl.ds(pl.multiple_of(q * slot, slot), slot), :].astype(jnp.float32)

    def remote(src, dst, s, r, device):
        return pltpu.make_async_remote_copy(src_ref=src, dst_ref=dst, send_sem=s, recv_sem=r,
                                            device_id=device, device_id_type=MESH)

    def send_d(k):
        return remote(going.at[(e + n - k) % n], at(rows, e, t), d_s.at[k], d_r.at[k],
                      ((e + n - k) % n, t))

    def send_a(k):
        s = (e + k) % n
        return remote(at(rows, s, t), at(rows, s, t), a_s.at[k], a_r.at[k], (e, pa))

    def send_b(k):
        s = (e + k) % n
        return remote(at(rows, s, t), at(rows, s, t), b_s.at[k], b_r.at[k], (e, pb))

    def send_c(k):
        s = (e + k) % n
        return remote(at(rows, s, pb), at(rows, s, pb), c_s.at[k], c_r.at[k], (e, pa))

    def send_ra(k, j):
        s = (e + k) % n
        return remote(at(rows, s, pa if j == 0 else pd), half.at[k, j], ra_s.at[k, j],
                      ra_r.at[k, j], (e, pa))

    def send_rb(k):
        return remote(half.at[k, 1], half.at[k, 2], rb_s.at[k], rb_r.at[k], (e, pb))

    def send_q(k):
        return remote(half.at[k, 0], back.at[e], q_s.at[k], q_r.at[k], ((e + k) % n, t))

    def send_t(d):
        return remote(tot_ref, tp_tot.at[t], t_s.at[d], t_r.at[d], (e, (t + d) % m))

    def send_e(k):
        return remote(grp, ep_tot.at[e], e_s.at[k], e_r.at[k], ((e + k) % n, t))

    values = tok_ref[...].astype(jnp.float32)
    center = jnp.mean(values, -1, keepdims=True)
    spread = jnp.mean(jnp.square(values - center), -1, keepdims=True)
    normed = ((values - center) * lax.rsqrt(spread + EPSILON) * gain_ref[...]).astype(jnp.bfloat16)
    count = values.shape[0]
    top = flat_ref.shape[0]
    place = lax.broadcasted_iota(jnp.int32, (n * slot, count), 0)
    pick = jnp.zeros((n * slot, count), jnp.float32)
    for k in range(top):
        pick = pick + jnp.where(place == flat_ref[k : k + 1, :], 1.0, 0.0)
    outgoing = jnp.dot(pick.astype(jnp.bfloat16), normed, preferred_element_type=jnp.float32)
    going[...] = outgoing.astype(jnp.bfloat16).reshape(going.shape)
    rows[e, pl.ds(pl.multiple_of(t * slot, slot), slot), :] = going[e]
    tp_tot[t] = tot_ref[...]

    pl.semaphore_wait(barrier, n - 1 + m - 1)

    def go(k, _):
        send_d(k).start()
        return 0

    for d in range(1, m):
        send_t(d).start()
    lax.fori_loop(1, n, go, 0)

    for d in range(1, m):
        send_t(d).wait_recv()
    total_f = tp_tot[0, 0:1, :]
    total_s = tp_tot[0, 1:2, :]
    for d in range(1, m):
        total_s = tp_tot[d, 0:1, :] * total_s + tp_tot[d, 1:2, :]
        total_f = total_f * tp_tot[d, 0:1, :]
    grp[0:1, :] = total_f
    grp[1:2, :] = total_s
    grp[2:, :] = jnp.zeros((grp.shape[0] - 2, grp.shape[1]), jnp.float32)
    ep_tot[e] = grp[...]

    def go_e(k, _):
        send_e(k).start()
        return 0

    lax.fori_loop(1, n, go_e, 0)
    for load in loads:
        load.wait()

    def step(i, _):
        @pl.when(i < n)
        def _():
            @pl.when(i > 0)
            def _():
                send_d(i).wait_recv()

            send_b(i).start()
            send_a(i).start()

        @pl.when((i >= 1) & (i < n + 1))
        def _():
            k = i - 1
            send_b(k).wait_recv()
            send_c(k).start()

        @pl.when((i >= 2) & (i < n + 2))
        def _():
            k = i - 2
            s = (e + k) % n
            send_a(k).wait_recv()
            send_c(k).wait_recv()
            x = rows[s]
            hidden = (jax.nn.silu(jnp.dot(x, wg[...], preferred_element_type=jnp.float32))
                      * jnp.dot(x, wu[...], preferred_element_type=jnp.float32)).astype(jnp.bfloat16)
            result = jnp.dot(hidden, wd[...], preferred_element_type=jnp.float32)
            send_a(k).wait_send()
            send_b(k).wait_send()
            send_c(k).wait_send()
            rows[s] = result.astype(jnp.bfloat16)
            send_ra(k, 1).start()
            send_ra(k, 0).start()

        @pl.when((i >= 3) & (i < n + 3))
        def _():
            k = i - 3
            s = (e + k) % n
            send_ra(k, 1).wait_recv()
            both = part(s, pb) + half[k, 1].astype(jnp.float32)
            half[k, 1] = both.astype(jnp.bfloat16)
            send_rb(k).start()

        @pl.when(i >= 4)
        def _():
            k = i - 4
            s = (e + k) % n
            send_ra(k, 0).wait_recv()
            send_rb(k).wait_recv()
            whole = part(s, t) + half[k, 0].astype(jnp.float32) + half[k, 2].astype(jnp.float32)
            half[k, 0] = whole.astype(jnp.bfloat16)

            @pl.when(k > 0)
            def _():
                send_q(k).start()

            @pl.when(k == 0)
            def _():
                back[e] = whole.astype(jnp.bfloat16)

        return 0

    lax.fori_loop(0, n + 4, step, 0)

    def finish(k, _):
        send_d(k).wait_send()
        send_e(k).wait()
        send_q(k).wait()
        return 0

    lax.fori_loop(1, n, finish, 0)

    def finish_local(k, _):
        send_ra(k, 0).wait_send()
        send_ra(k, 1).wait_send()
        send_rb(k).wait_send()
        return 0

    lax.fori_loop(0, n, finish_local, 0)
    for d in range(1, m):
        send_t(d).wait_send()

    carried = jnp.zeros((1, grp.shape[1]), jnp.float32)

    def over(k, carried):
        new = ep_tot[k, 0:1, :] * carried + ep_tot[k, 1:2, :]
        return jnp.where(k < e, new, carried)

    carried = lax.fori_loop(0, n, over, carried)
    for d in range(m):
        new = tp_tot[d, 0:1, :] * carried + tp_tot[d, 1:2, :]
        carried = jnp.where(d < t, new, carried)
    carry_ref[...] = jnp.broadcast_to(carried, carry_ref.shape)

    results = back[...].reshape(n * slot, back.shape[2])
    place = lax.broadcasted_iota(jnp.int32, (count, n * slot), 1)
    summed = jnp.zeros(out_ref.shape, jnp.float32)
    for k in range(top):
        pick = jnp.where(place == flat_t_ref[:, k : k + 1], 1.0, 0.0).astype(jnp.bfloat16)
        picked = jnp.dot(pick, results, preferred_element_type=jnp.float32)
        summed = summed + picked * weight_ref[:, k : k + 1]
    out_ref[...] = summed.astype(jnp.bfloat16)


def experts(n, m, slot, tokens, gain, flat, route_weight, totals, w_gate, w_up, w_down):
    count, width = tokens.shape
    hidden = w_gate.shape[1]
    dma = lambda *shape: pltpu.SemaphoreType.DMA(shape)
    vmem = pl.BlockSpec(memory_space=pltpu.VMEM)
    anyw = pl.BlockSpec(memory_space=pl.ANY)
    bf = jnp.bfloat16
    return pl.pallas_call(
        functools.partial(expert_kernel, n, m, slot),
        in_specs=[vmem] * 6 + [anyw] * 3,
        out_specs=[vmem] * 2,
        out_shape=[jax.ShapeDtypeStruct((count, width), bf), jax.ShapeDtypeStruct((8, width), jnp.float32)],
        scratch_shapes=[
            pltpu.VMEM((width, hidden), bf), pltpu.VMEM((width, hidden), bf),
            pltpu.VMEM((hidden, width), bf),
            pltpu.VMEM((n, slot, width), bf), pltpu.VMEM((n, m * slot, width), bf),
            pltpu.VMEM((n, 3, slot, width), bf), pltpu.VMEM((n, slot, width), bf),
            pltpu.VMEM((m, 8, width), jnp.float32), pltpu.VMEM((8, width), jnp.float32),
            pltpu.VMEM((n, 8, width), jnp.float32),
            dma(3)] + [dma(n)] * 8 + [dma(n, 2)] * 2 + [dma(n)] * 4 + [dma(m)] * 2 + [dma(n)] * 2,
        compiler_params=pltpu.CompilerParams(
            collective_id=0, has_side_effects=True, vmem_limit_bytes=63 * 1024 * 1024),
    )(tokens, gain, flat.T, flat, route_weight, totals, w_gate, w_up, w_down)


def shards(
    gate_branch,
    rec_branch,
    conv_weight,
    gate_a,
    gate_x,
    decay_param,
    decay_shift,
    tokens,
    routes,
    route_weight,
    norm_gain,
    w_gate,
    w_up,
    w_down,
):
    tap_count = conv_weight.shape[0]
    row_count, width_all = rec_branch.shape
    n, m = lax.axis_size("ep"), lax.axis_size("tp")
    previous = passed_along(rec_branch[row_count - (tap_count - 1) :], ("ep", "tp"), 1)
    lead = -(tap_count - 1) % 8
    previous = jnp.pad(previous.astype(jnp.float32), ((lead, 0), (0, 0)))
    rate = 8.0 * jax.nn.softplus(-decay_param)
    factor, state = local_mixer(
        previous, rec_branch, conv_weight, gate_a, gate_x, rate[None, :], decay_shift[:, None]
    )
    totals = jnp.concatenate(
        [factor[-1:], state[-1:], jnp.zeros((6, width_all), jnp.float32)], 0
    )
    block_rows, top_count = routes.shape
    capacity = max(2, block_rows * top_count * 5 // (4 * n))
    slot = -(-capacity // 16) * 16
    flat = routes * slot + slot_numbers(routes, block_rows, n)
    expert_out, carried = experts(
        n, m, slot, tokens, norm_gain[None, :], flat, route_weight, totals,
        w_gate[0], w_up[0], w_down[0],
    )
    states = state + factor * carried[0:1]
    mixed_out = (states * jax.nn.gelu(gate_branch.astype(jnp.float32), approximate=True)).astype(
        jnp.bfloat16
    )
    return (mixed_out, expert_out)


def solution(mesh):
    in_specs = (
        P(("ep", "tp"), None),
        P(("ep", "tp"), None),
        P(),
        P(),
        P(),
        P(),
        P(("ep", "tp")),
        P(("ep", "tp"), None),
        P(("ep", "tp"), None),
        P(("ep", "tp"), None),
        P(),
        P("ep", None, "tp"),
        P("ep", None, "tp"),
        P("ep", "tp", None),
    )
    out_specs = (P(("ep", "tp"), None), P(("ep", "tp"), None))
    return jax.shard_map(shards, mesh=mesh, in_specs=in_specs, out_specs=out_specs, check_vma=False)
```

time: 320 us -> 140 us (0.44)
  Pallas kernels: 0 us -> 119 us
  blocking collectives: 117 us -> 0 us
  local copies, waits for them, and re-layouts: 75.2 us -> 10.1 us
  waiting for transfers between devices: 46.9 us -> 0.01 us
  matrix products: 30.9 us -> 0 us
  other arithmetic: 26 us -> 6.86 us
  between operations: 14.4 us -> 0.7 us
    pallas_call x0 -> x2, Pallas kernels: none -> 119 us  [the longest x1 111 us: experts(): pl.pallas_call(functools.partial(expert_kernel, n, m, slot), in_specs=[vm...]
    all_gather x2 -> x0, blocking collectives: 78.7 us -> none  [prefix(): gathered = jax.tree.map(lambda a: lax.all_gather(a, axis), part)]
    dynamic_update_slice x32 -> x0, local copies, waits for them, and re-layouts: 47.7 us -> none  [blocked_recurrence(): _, before = lax.scan(carry_step, start, (factors[-1], states[-1]))]
    all_to_all x1 -> x0, blocking collectives: 38.6 us -> none  [shards(): lax.all_to_all(outgoing, 'ep', split_axis=0, concat_axis=0, tiled=True)]
    dot_general x4 -> x0, matrix products: 30.9 us -> none  [the longest x1 17.5 us: shards(): jnp.dot(hidden, w_down[0], preferred_element_type=jnp.float32)]
    all_to_all x1 -> x0, waiting for transfers between devices: 29.4 us -> none  [shards(): lax.all_to_all(route_out.reshape(ep_count, capacity, width_all), 'ep', sp...]
    all_gather x1 -> x0, waiting for transfers between devices: 17.5 us -> none  [shards(): lax.all_gather(arrived.reshape(-1, width_all), 'tp', axis=0, tiled=True)]
    reduce_sum x3 -> x0, other arithmetic: 7.44 us -> none  [the longest x1 4.92 us: shards(): jnp.sum(picked * route_weight[:, :, None], axis=1).astype(jnp.bfloat16)]
  transfers between devices with their start and end apart: 4 -> 1, of which waited for: 2 -> 0; matrix products, arithmetic and copies ran while one was open for 27% -> 5% of each run, Pallas kernels for 0% -> 0%
where the time goes in v1:
time: 140 us; the launch traced here: 139 us
  Pallas kernels  119 us (85%)
  local copies, waits for them, and re-layouts  10.1 us (7%)
  other arithmetic  6.86 us (5%)
  starting transfers between devices  2.4 us (2%)
    pallas_call x1, Pallas kernels, experts(): pl.pallas_call(functools.partial(expert_kernel, n, m, slot), in_specs=[vm...  111 us
    pallas_call x1, Pallas kernels, local_mixer(): pl.pallas_call(mixer_kernel, grid=(blocks,), in_specs=[col(prev.shape[0])...  7.97 us
    unnamed x7, local copies, waits for them, and re-layouts  4.07 us
  transfers between devices with their start and end apart: 1, of which 0 were waited for; matrix products, arithmetic and copies ran while one was open for 5% of the time, Pallas kernels for 0%

profile of v1, /device:TPU:0, one launch (start us, length us, event | category | flops | bytes accessed | tf_op | source)
XLA Modules:
  0.0 138.9 jit_solution(2660664800276557474)
XLA Ops:
  0.6 0.8 slice.18
  1.4 2.4 %collective-permute-start = (bf16[3,2048]{1,0:T(4,128)(2,1)S(1)}, bf16[3,2048]{1,0:T(4,128)(2,1)S(1)}, u32[]{:S(2)}, u32[]{:S(2)}) collective-permute-start(bf16[3,2048]{1,0:T(4,128)(2,1)S(1)} %slice.18), channel_id=1, source_target_pairs={{0,1},{1,2},{2,3},{3,4},{4,5},{5,6},{6,7},{7,8},{8,9},{9,10},{10,1... | collective-permute-start | bytes 36872 | tf_op jit(solution)/shard_map/ppermute | solution.py:17
  3.8 0.7 broadcast_multiply_fusion
  4.5 0.8 copy.28
  5.3 1.3 fusion.7
  6.6 0.1 eq.26
  6.7 0.6 reduce-window.6
  7.3 0.2 slice_reduce_fusion
  7.6 0.1 fusion.8
  7.7 0.1 copy.29
  7.8 1.4 %copy.27.shift_ref = f32[128,1]{1,0:T(8,128)} copy(f32[128,1]{0,1:T(1,128)} %bitcast.35) | data formatting | bytes 1024 | tf_op jit(solution)/shard_map/broadcast_in_dim | solution.py:344
  9.2 1.4 %copy.31.weight_ref = f32[128,2]{1,0:T(8,128)} copy(f32[128,2]{0,1:T(2,128)} %param.23) | data formatting | bytes 2048 | tf_op args[9]
  10.6 0.1 reduce_sum.12
  10.7 0.0 copy-start
  10.8 0.7 copy.30.flat_ref
  11.4 0.1 pad.10.clone
  11.5 0.0 collective-permute-done
  11.5 0.6 pad_convert_fusion.prev_ref
  12.1 8.0 %shard_map.149 = (f32[128,2048]{1,0:T(8,128)}, f32[128,2048]{1,0:T(8,128)}) custom-call(f32[8,2048]{1,0:T(8,128)} %pad_convert_fusion.prev_ref, bf16[128,2048]{1,0:T(8,128)(2,1)} %rec_ref.1, f32[4,2048]{1,0:T(4,128)} %conv_ref.1, bf16[8,256,256]{2,1,0:T(8,128)(2,1)} %ga_ref.1, bf16[8,256,256]{2,1,0:T(8,128)(2,1)} %gx_ref.1, f32[1,2048]{1,0:T(1,128)} %bitcast.31, ...), custom_call_target="tpu_custom_call" | custom-call | tf_op jit(solution)/shard_map/pallas_call | solution.py:69
  20.1 0.8 slice.22
  20.9 0.8 slice.21
  21.8 0.7 maximum_maximum_fusion.tot_ref
  22.5 0.0 copy-done
  22.5 0.0 copy-start.1
  22.5 110.9 %shard_map.150 = (bf16[128,2048]{1,0:T(8,128)(2,1)}, f32[8,2048]{1,0:T(8,128)}) custom-call(bf16[128,2048]{1,0:T(8,128)(2,1)} %tok_ref.1, f32[1,2048]{1,0:T(1,128)} %bitcast.33, s32[2,128]{1,0:T(2,128)} %copy.30.flat_ref, s32[128,2]{1,0:T(8,128)} %copy-done, f32[128,2]{1,0:T(8,128)} %copy.31.weight_ref, f32[8,2048]{1,0:T(8,128)} %maximum_maximum_fusion.tot_ref, ...), custom_call_target="tpu_custom_call" | custom-call | tf_op jit(solution)/shard_map/pallas_call | solution.py:302
  133.4 0.8 slice.23
  134.3 0.0 copy-done.1
  134.3 2.8 %fusion.6 = bf16[128,2048]{1,0:T(8,128)(2,1)} fusion(bf16[128,2048]{1,0:T(8,128)(2,1)S(1)} %copy-done.1, f32[128,2048]{1,0:T(8,128)} %get-tuple-element.6, f32[128,2048]{1,0:T(8,128)} %get-tuple-element.7, f32[2048]{0:T(1024)S(1)} %bitcast.32), kind=kLoop, calls=%fused_computation.10 | loop fusion | flops 3407872 | bytes 3153920 | tf_op jit(solution)/shard_map/convert_element_type | solution.py:358
  137.1 1.9 %copy.33 = bf16[128,2048]{1,0:T(8,128)(2,1)} copy(bf16[128,2048]{1,0:T(8,128)(2,1)} %get-tuple-element.13) | data formatting | bytes 1048576
  (5 shorter events, 0.1 us)
Async XLA Ops:
  1.4 10.1 %collective-permute-start = (bf16[3,2048]{1,0:T(4,128)(2,1)S(1)}, bf16[3,2048]{1,0:T(4,128)(2,1)S(1)}, u32[]{:S(2)}, u32[]{:S(2)}) collective-permute-start(bf16[3,2048]{1,0:T(4,128)(2,1)S(1)} %slice.18), channel_id=1, source_target_pairs={{0,1},{1,2},{2,3},{3,4},{4,5},{5,6},{6,7},{7,8},{8,9},{9,10},{10,1... | collective-permute-start | bytes 36872 | tf_op jit(solution)/shard_map/ppermute | solution.py:17
  10.7 11.8 %copy-start = (s32[128,2]{1,0:T(8,128)}, s32[128,2]{1,0:T(8,128)S(1)}, u32[]{:S(2)}) copy-start(s32[128,2]{1,0:T(8,128)S(1)} %add.24.flat_t_ref) | copy-start | bytes 3076
  22.5 111.8 %copy-start.1 = (bf16[128,2048]{1,0:T(8,128)(2,1)S(1)}, bf16[128,2048]{1,0:T(8,128)(2,1)}, u32[]{:S(2)}) copy-start(bf16[128,2048]{1,0:T(8,128)(2,1)} %param.14) | copy-start | bytes 1572868
